TPU v7x, 256 devices: a whole 4x4x8 slice. The times are simulated.
256 devices in a mesh: ep: 16 (over y, x), tp: 16 (over z, core).
Axes of the slice: x: 4, y: 4, z: 8, core: 2. Of those that a mesh axis runs over, the one named last changes fastest.
Arguments:
- tokens: bfloat16 [256, 2048], P('ep', 'tp'), may hold values from -6 to 6
- key_cache: bfloat16 [256, 16, 1024, 128], P('ep', 'tp'), may hold values from -1700 to 1700
- value_cache: bfloat16 [256, 16, 1024, 128], P('ep', 'tp'), may hold values from -6 to 6
- gate_totals: float32 [256, 16, 1024], P('ep', 'tp'), as said below
- lengths: int32 [256], P('ep'), may hold values from 128 to 1024
- attn_gain: float32 [2048], replicated, may hold values from 0.1 to 1.9
- w_query: bfloat16 [2048, 2048], P(None, 'tp'), may hold values from -0.125 to 0.125
- w_key: bfloat16 [2048, 2048], P(None, 'tp'), may hold values from -0.125 to 0.125
- w_value: bfloat16 [2048, 2048], P(None, 'tp'), may hold values from -0.125 to 0.125
- w_forget: bfloat16 [2048, 16], replicated, may hold values from -0.125 to 0.125
- forget_bias: float32 [16], replicated, may hold values from -3 to 0
- w_attn_out: bfloat16 [2048, 2048], P('tp'), may hold values from -0.1875 to 0.1875
- moe_gain: float32 [2048], replicated, may hold values from 0.1 to 1.9
- group_ids: int32 [256, 1], P('ep'), may hold values from 0 to 15; in each aligned block of 16 rows (0 to 15, 16 to 31, ...) at most 2 rows name the same one
- inner_ids: int32 [256, 2], P('ep'), may hold values from 0 to 3, all different within a row
- group_prob: float32 [256], P('ep'), may hold values from 0.2 to 1
- pair_logits: float32 [256, 2], P('ep'), may hold values from -6 to 6
- w_expert_gate: bfloat16 [16, 2048, 2048], P('ep', None, 'tp'), may hold values from -0.125 to 0.125
- w_expert_up: bfloat16 [16, 2048, 2048], P('ep', None, 'tp'), may hold values from -0.125 to 0.125
- w_expert_down: bfloat16 [16, 2048, 2048], P('ep', 'tp'), may hold values from -0.375 to 0.375
- w_dense_in: bfloat16 [2048, 2048], P(None, 'tp'), may hold values from -0.125 to 0.125
- w_dense_out: bfloat16 [2048, 2048], P('tp'), may hold values from -0.1875 to 0.1875
- dense_gate: float32 [2048], P('tp'), may hold values from -2 to 2
Outputs:
- layer_output: bfloat16 [256, 2048], P('ep', 'tp')
- new_keys: bfloat16 [256, 16, 128], P('ep', 'tp')
- new_values: bfloat16 [256, 16, 128], P('ep', 'tp')
- new_gates: float32 [256, 16], P('ep', 'tp')
Inputs may be any that keep to these rules, and one draw needn't show every extreme that they name: `group_ids`: within the 16 sequences of each index of ep (aligned blocks of rows), no group is named by more than 2 sequences, a bound that some block reaches. `inner_ids`: each row names 2 different experts of its group. `gate_totals`: along positions the values of each sequence and head never rise.
All inputs are finite; a program needn't handle non-finite values.
Results may differ from a plain program's by a relative error of at most 0.011.
Values may be sent and summed in bfloat16 or wider, within the bound.
A program may use at most 64 MiB of HBM per device.

v0:
```python
import jax
import jax.numpy as jnp
from jax import lax
from jax.sharding import PartitionSpec as P

FFE = 512
EPG = 4
EPS = 1e-06
FLOOR = -1e30


def split_up(array, dim, size):
    dims = array.shape
    pieces = array.reshape(*dims[:dim], size, dims[dim] // size, *dims[dim + 1 :])
    return jnp.moveaxis(pieces, dim, 0)


def sum_at_owner(array, axis, dim):
    size = lax.axis_size(axis)
    pieces = lax.all_to_all(split_up(array, dim, size), axis, 0, 0, tiled=True)
    return jnp.sum(pieces, axis=0)


def joined_along(pieces, dim):
    dims = list(pieces.shape[1:])
    dims[dim] *= pieces.shape[0]
    return jnp.moveaxis(pieces, 0, dim).reshape(dims)


def copy_for_each(array, axis):
    copies = jnp.broadcast_to(array, (lax.axis_size(axis), *array.shape))
    return lax.all_to_all(copies, axis, split_axis=0, concat_axis=0, tiled=True)


def gathered_copies(array, axis, dim):
    return joined_along(copy_for_each(array, axis), dim)


def side_by_side(arrays, axis, split_dim, concat_dim, along):
    both = jnp.concatenate(arrays, axis=along)
    filled, at, gathered = (
        lax.all_to_all(both, axis, split_axis=split_dim, concat_axis=concat_dim, tiled=True),
        0,
        [],
    )
    for a in arrays:
        gathered.append(lax.slice_in_dim(filled, at, at + a.shape[along], axis=along))
        at += a.shape[along]
    return tuple(gathered)


def sent_together(arrays, axis, dim, along):
    widths = [a.shape[along] for a in arrays]
    both = jnp.concatenate(arrays, axis=along)
    filled = sum_at_owner(both, axis, dim)
    return tuple(jnp.split(filled, [sum(widths[:k]) for k in range(1, len(widths))], axis=along))


def norm_rows(row_data, gain_vec):
    values = row_data.astype(jnp.float32)
    factor = lax.rsqrt(jnp.mean(values * values, axis=-1, keepdims=True) + EPS)
    return (values * factor * gain_vec).astype(jnp.bfloat16)


def head_norm(values):
    factor = lax.rsqrt(jnp.mean(values * values, axis=-1, keepdims=True) + EPS)
    return (values * factor).astype(jnp.bfloat16)


def attend(queries, fresh_key, fresh_value, key_cache, value_cache, gate_totals, lengths, current):
    score_scale = queries.shape[-1] ** (-0.5)
    scores = (
        jnp.einsum("shd,shld->shl", queries, key_cache, preferred_element_type=jnp.float32)
        * score_scale
    )
    scores = scores + current[:, :, None] - gate_totals
    entry_indices = jnp.arange(key_cache.shape[2])
    live_mask = (entry_indices[None, :] < lengths[:, None])[:, None, :]
    scores = jnp.where(live_mask, scores, FLOOR)
    own_score = (
        jnp.sum(queries.astype(jnp.float32) * fresh_key.astype(jnp.float32), axis=-1) * score_scale
    )
    peak = jnp.maximum(jnp.max(scores, axis=-1), own_score)
    expo_terms = jnp.where(live_mask, jnp.exp(scores - peak[:, :, None]), 0.0)
    own_expo = jnp.exp(own_score - peak)
    denom_sum = jnp.sum(expo_terms, axis=-1) + own_expo
    weights = (expo_terms / denom_sum[:, :, None]).astype(jnp.bfloat16)
    own_weight = (own_expo / denom_sum).astype(jnp.bfloat16)
    attended = jnp.einsum("shl,shld->shd", weights, value_cache, preferred_element_type=jnp.float32)
    attended = attended + own_weight.astype(jnp.float32)[:, :, None] * fresh_value.astype(
        jnp.float32
    )
    return attended.astype(jnp.bfloat16)


def body(
    tokens,
    key_cache,
    value_cache,
    gate_totals,
    lengths,
    attn_gain,
    w_query,
    w_key,
    w_value,
    w_forget,
    forget_bias,
    w_attn_out,
    moe_gain,
    group_ids,
    inner_ids,
    group_prob,
    pair_logits,
    w_expert_gate,
    w_expert_up,
    w_expert_down,
    w_dense_in,
    w_dense_out,
    dense_gate,
):
    gathered = lax.all_gather(tokens, "tp", axis=1, tiled=True)
    normed = norm_rows(gathered, attn_gain)
    seq_count = gathered.shape[0]
    heads_dev = key_cache.shape[1]
    head_dim = key_cache.shape[3]

    def project(weight):
        return jnp.dot(normed, weight, preferred_element_type=jnp.float32).reshape(
            seq_count, heads_dev, head_dim
        )

    queries = head_norm(project(w_query))
    new_keys = head_norm(project(w_key))
    new_values = project(w_value).astype(jnp.bfloat16)
    first_head = lax.axis_index("tp") * heads_dev
    forget_cols = lax.dynamic_slice_in_dim(w_forget, first_head, heads_dev, 1)
    forget_shift = lax.dynamic_slice_in_dim(forget_bias, first_head, heads_dev, 0)
    log_gate = jax.nn.log_sigmoid(
        jnp.dot(normed, forget_cols, preferred_element_type=jnp.float32) + forget_shift
    )
    entry_indices = jnp.arange(gate_totals.shape[2])
    at_last = (entry_indices[None, :] == (lengths - 1)[:, None])[:, None, :]
    new_gates = jnp.sum(jnp.where(at_last, gate_totals, 0.0), axis=2) + log_gate
    attended = attend(
        queries, new_keys, new_values, key_cache, value_cache, gate_totals, lengths, new_gates
    )
    partial_value = jnp.dot(
        attended.reshape(seq_count, heads_dev * head_dim),
        w_attn_out,
        preferred_element_type=jnp.float32,
    )
    piece_sum = sum_at_owner(partial_value, "tp", 1)
    own_residual = (tokens.astype(jnp.float32) + piece_sum).astype(jnp.bfloat16)
    moe_in = norm_rows(gathered_copies(own_residual, "tp", 1), moe_gain)
    groups = lax.axis_size("ep")
    capacity = max(2, 2 * seq_count // groups)
    first_share = jax.nn.sigmoid(pair_logits[:, 0] - pair_logits[:, 1])
    pair_share = group_prob[:, None] * jnp.stack([first_share, 1.0 - first_share], axis=1)
    inner_range = jnp.arange(EPG)
    spread = jnp.sum(
        jnp.where(inner_ids[:, :, None] == inner_range[None, None, :], pair_share[:, :, None], 0.0),
        axis=1,
    ).astype(jnp.bfloat16)
    choose = (group_ids == jnp.arange(groups)[None, :]).astype(jnp.int32)
    before = jnp.cumsum(choose, axis=0) - choose
    slot_of = group_ids[:, 0] * capacity + jnp.sum(before * choose, axis=1)
    slot_ids = jnp.arange(groups * capacity)
    send_map = (slot_of[None, :] == slot_ids[:, None]).astype(jnp.bfloat16)
    send_weights = jnp.dot(send_map, spread, preferred_element_type=jnp.float32).astype(
        jnp.bfloat16
    )
    send_rows = jnp.dot(send_map, moe_in, preferred_element_type=jnp.float32).astype(jnp.bfloat16)
    recv_rows, recv_weights = side_by_side((send_rows, send_weights), "ep", 0, 0, 1)
    dense_hidden = jax.nn.silu(
        jnp.dot(moe_in, w_dense_in, preferred_element_type=jnp.float32)
    ).astype(jnp.bfloat16)
    dense_part = jnp.dot(dense_hidden, w_dense_out, preferred_element_type=jnp.float32)
    hidden_dev = w_expert_gate.shape[2]
    expert_index = lax.axis_index("tp") * hidden_dev // FFE
    route_col = jnp.sum(
        jnp.where(inner_range[None, :] == expert_index, recv_weights.astype(jnp.float32), 0.0),
        axis=1,
    )
    gate_pre = jnp.dot(recv_rows, w_expert_gate[0], preferred_element_type=jnp.float32)
    up_pre = jnp.dot(recv_rows, w_expert_up[0], preferred_element_type=jnp.float32)
    hidden = (jax.nn.silu(gate_pre) * up_pre * route_col[:, None]).astype(jnp.bfloat16)
    expert_part = jnp.dot(hidden, w_expert_down[0], preferred_element_type=jnp.float32)
    expert_sum, dense_sum = sent_together((expert_part, dense_part), "tp", 1, 0)
    returned = lax.all_to_all(
        expert_sum.astype(jnp.bfloat16), "ep", split_axis=0, concat_axis=0, tiled=True
    )
    expert_out = lax.dot_general(
        send_map, returned, (((0,), (0,)), ((), ())), preferred_element_type=jnp.float32
    )
    layer_output = (
        own_residual.astype(jnp.float32) + expert_out + jax.nn.sigmoid(dense_gate) * dense_sum
    )
    return (layer_output.astype(jnp.bfloat16), new_keys, new_values, new_gates)


def solution(mesh):
    placed = (
        P("ep", "tp"),
        P("ep", "tp", None, None),
        P("ep", "tp", None, None),
        P("ep", "tp", None),
        P("ep"),
        P(),
        P(None, "tp"),
        P(None, "tp"),
        P(None, "tp"),
        P(),
        P(),
        P("tp", None),
        P(),
        P("ep", None),
        P("ep", None),
        P("ep"),
        P("ep", None),
        P("ep", None, "tp"),
        P("ep", None, "tp"),
        P("ep", "tp", None),
        P(None, "tp"),
        P("tp", None),
        P("tp"),
    )
    return jax.shard_map(
        body,
        mesh=mesh,
        in_specs=placed,
        out_specs=(P("ep", "tp"), P("ep", "tp", None), P("ep", "tp", None), P("ep", "tp")),
        check_vma=False,
    )
```

profile of v0, /device:TPU:1, one launch (start us, length us, event | category | flops | bytes accessed | tf_op | source)
XLA Modules:
  0.0 108.0 jit_solution(13230268292263461012)
XLA Ops:
  0.7 21.8 %all_gather.3 = bf16[16,2048]{1,0:T(8,128)(2,1)S(1)} all-gather(bf16[16,128]{1,0:T(8,128)(2,1)} %param.23), channel_id=1, replica_groups=mesh['ep'=16,'tp'=16] {'tp'}, dimensions={1}, use_global_device_ids=true | all-gather | bytes 69632 | tf_op jit(solution)/shard_map/all_gather | solution.py:121
  22.7 1.4 %multiply_reduce_fusion.1 = (f32[16]{0:T(128)S(1)}, f32[16,128]{1,0:T(8,128)S(1)}) fusion(bf16[2048,128]{1,0:T(8,128)(2,1)} %param.30, bf16[16,2048]{1,0:T(8,128)(2,1)S(1)} %all_gather.3, f32[2048]{0:T(1024)} %param.28, f32[16]{0:T(128)S(1)} %add_rsqrt_fusion.3), kind=kOutput, calls=%fused_computation.71 | convolution fusion | flops 8523760 | bytes 606336 | tf_op jit(solution)/shard_map/dot_general | solution.py:128
  24.1 1.4 %multiply_reduce_fusion.2 = (f32[16]{0:T(128)S(1)}, f32[16,128]{1,0:T(8,128)S(1)}) fusion(bf16[2048,128]{1,0:T(8,128)(2,1)} %param.29, bf16[16,2048]{1,0:T(8,128)(2,1)S(1)} %all_gather.3, f32[2048]{0:T(1024)} %param.28, f32[16]{0:T(128)S(1)} %add_rsqrt_fusion.3), kind=kOutput, calls=%fused_computation.74 | convolution fusion | flops 8523760 | bytes 606336 | tf_op jit(solution)/shard_map/dot_general | solution.py:128
  25.5 0.7 broadcast_add_fusion
  26.2 0.8 fusion.59
  27.0 3.4 %fusion.2 = f32[16,1,1024]{2,1,0:T(1,128)S(1)} fusion(bf16[16,1,1024,128]{3,2,1,0:T(8,128)(2,1)} %param.24, bf16[16,128,1]{1,0,2:T(8,128)(2,1)S(1)} %get-tuple-element.10), kind=kOutput, calls=%fused_computation.2 | convolution fusion | flops 4194304 | bytes 4263936 | tf_op jit(solution)/shard_map/shd,shld->shl/dot_general | solution.py:73
  30.4 0.6 dynamic_slice.7
  31.0 0.3 fusion.29
  31.3 1.6 %fusion.51 = f32[16]{0:T(128)S(1)} fusion(f32[16]{0:T(128)S(1)} %fusion.29, bf16[2048,16]{0,1:T(8,128)(2,1)} %param.32, s32[]{:T(128)S(6)} %select_n.34, f32[]{:T(128)} %bitcast.4, bf16[16,2048]{1,0:T(8,128)(2,1)S(1)} %all_gather.3, f32[2048]{0:T(1024)S(1)} %copy-done.8, f32[16]{0:T(128)S(1)} %add_rsqrt_fusion.3), kind=kOutput, calls=%fused_computation.85 | convolution fusion | flops 196768 | bytes 82628 | tf_op jit(solution)/shard_map/dot_general | solution.py:139
  33.0 0.3 fusion.74
  33.4 0.3 fusion.73
  33.7 0.2 convolution_convert_fusion.1
  34.0 0.3 copy.53
  34.3 3.0 %fusion = f32[16,1,128]{2,1,0:T(1,128)S(1)} fusion(bf16[16,1,1024,128]{3,2,1,0:T(8,128)(2,1)} %param.25, f32[16]{0:T(128)S(1)} %get-tuple-element.12, f32[16,1,1024]{2,1,0:T(1,128)S(1)} %get-tuple-element.7, f32[16]{0:T(128)S(1)} %multiply_maximum_fusion, s32[16]{0:T(128)S(1)} %copy-done.12), kind=kOutput, calls=%fused_computation | convolution fusion | flops 4276224 | bytes 4268224 | tf_op jit(solution)/shard_map/shl,shld->shd/dot_general | solution.py:89
  37.3 0.9 convolution_bitcast_fusion
  38.3 3.8 %all-to-all-start = ((f32[16,16,128]{2,1,0:T(8,128)}), f32[16,16,128]{2,1,0:T(8,128)S(1)}, u32[]{:S(2)}, u32[]{:S(2)}) async-start(f32[16,16,128]{2,1,0:T(8,128)} %convolution_bitcast_fusion), calls=%async_computation | async-start | bytes 262144 | tf_op jit(solution)/shard_map/all_to_all | solution.py:20
  42.5 8.5 %all-to-all-done = f32[16,16,128]{2,1,0:T(8,128)S(1)} async-done(((f32[16,16,128]{2,1,0:T(8,128)}), f32[16,16,128]{2,1,0:T(8,128)S(1)}, u32[]{:S(2)}, u32[]{:S(2)}) %all-to-all-start) | async-done | bytes 131104 | tf_op jit(solution)/shard_map/all_to_all | solution.py:20
  51.0 0.6 broadcast_in_dim.32
  51.6 3.4 %all-to-all-start.1 = ((bf16[16,16,128]{2,1,0:T(8,128)(2,1)}), bf16[16,16,128]{2,1,0:T(8,128)(2,1)S(1)}, u32[]{:S(2)}, u32[]{:S(2)}) async-start(bf16[16,16,128]{2,1,0:T(8,128)(2,1)} %broadcast_in_dim.32), calls=%async_computation.1 | async-start | bytes 131072 | tf_op jit(solution)/shard_map/all_to_all | solution.py:32
  55.3 7.2 %all-to-all-done.1 = bf16[16,16,128]{2,1,0:T(8,128)(2,1)S(1)} async-done(((bf16[16,16,128]{2,1,0:T(8,128)(2,1)}), bf16[16,16,128]{2,1,0:T(8,128)(2,1)S(1)}, u32[]{:S(2)}, u32[]{:S(2)}) %all-to-all-start.1) | async-done | bytes 65568 | tf_op jit(solution)/shard_map/all_to_all | solution.py:32
  62.6 0.2 convolution_convert_fusion
  62.9 0.7 all_to_all.27
  63.6 6.8 %all-to-all-start.2 = ((bf16[16,2,2052]{2,1,0:T(2,128)(2,1)}), bf16[16,2,2052]{2,1,0:T(2,128)(2,1)S(1)}, u32[]{:S(2)}, u32[]{:S(2)}) async-start(bf16[16,2,2052]{2,1,0:T(2,128)(2,1)} %all_to_all.27), calls=%async_computation.2 | async-start | bytes 278528 | tf_op jit(solution)/shard_map/all_to_all | solution.py:42
  70.4 0.4 fusion.44
  70.8 6.4 %all-to-all-done.2 = bf16[16,2,2052]{2,1,0:T(2,128)(2,1)S(1)} async-done(((bf16[16,2,2052]{2,1,0:T(2,128)(2,1)}), bf16[16,2,2052]{2,1,0:T(2,128)(2,1)S(1)}, u32[]{:S(2)}, u32[]{:S(2)}) %all-to-all-start.2) | async-done | bytes 131360 | tf_op jit(solution)/shard_map/all_to_all | solution.py:42
  77.5 0.2 fusion.14
  77.7 0.4 fusion.6
  78.1 18.6 %all_to_all.39 = f32[16,48,128]{2,1,0:T(8,128)S(1)} all-to-all(f32[16,48,128]{2,1,0:T(8,128)S(1)} %bitcast_bitcast_fusion), channel_id=1, replica_groups=mesh['ep'=16,'tp'=16] {'tp'}, dimensions={0} | all-to-all | bytes 786432 | tf_op jit(solution)/shard_map/all_to_all | solution.py:20
  96.8 0.6 split.15
  97.4 3.5 %all-to-all-start.4 = ((bf16[16,2,128]{2,1,0:T(2,128)(2,1)}), bf16[16,2,128]{2,1,0:T(2,128)(2,1)S(1)}, u32[]{:S(2)}, u32[]{:S(2)}) async-start(bf16[16,2,128]{2,1,0:T(2,128)(2,1)} %bitcast.19), calls=%async_computation.4 | async-start | bytes 16384 | tf_op jit(solution)/shard_map/all_to_all | solution.py:189
  100.9 6.3 %all-to-all-done.4 = bf16[16,2,128]{2,1,0:T(2,128)(2,1)S(1)} async-done(((bf16[16,2,128]{2,1,0:T(2,128)(2,1)}), bf16[16,2,128]{2,1,0:T(2,128)(2,1)S(1)}, u32[]{:S(2)}, u32[]{:S(2)}) %all-to-all-start.4) | async-done | bytes 8224 | tf_op jit(solution)/shard_map/all_to_all | solution.py:189
  107.3 0.8 fusion.8
  (66 shorter events, 1.4 us)
Async XLA Ops:
  0.6 77.0 %copy-start = (bf16[1,128,2048]{2,1,0:T(8,128)(2,1)S(1)}, bf16[1,128,2048]{2,1,0:T(8,128)(2,1)}, u32[]{:S(2)}) copy-start(bf16[1,128,2048]{2,1,0:T(8,128)(2,1)} %param.42) | copy-start | bytes 1572868
  0.6 30.7 %copy-start.8 = (f32[2048]{0:T(1024)S(1)}, f32[2048]{0:T(1024)}, u32[]{:S(2)}) copy-start(f32[2048]{0:T(1024)} %param.28) | copy-start | bytes 24580
  0.7 32.4 %copy-start.12 = (s32[16]{0:T(128)S(1)}, s32[16]{0:T(128)}, u32[]{:S(2)}) copy-start(s32[16]{0:T(128)} %param.27) | copy-start | bytes 196
  0.7 29.7 %copy-start.18 = (f32[16]{0:T(128)S(1)}, f32[16]{0:T(128)}, u32[]{:S(2)}) copy-start(f32[16]{0:T(128)} %param.33) | copy-start | bytes 196
  0.7 30.3 %copy-start.7 = (f32[16,1,1024]{2,1,0:T(1,128)S(1)}, f32[16,1,1024]{2,1,0:T(1,128)}, u32[]{:S(2)}) copy-start(f32[16,1,1024]{2,1,0:T(1,128)} %param.26) | copy-start | bytes 196612
  0.7 33.0 %copy-start.1 = (bf16[2048,128]{1,0:T(8,128)(2,1)S(1)}, bf16[2048,128]{1,0:T(8,128)(2,1)}, u32[]{:S(2)}) copy-start(bf16[2048,128]{1,0:T(8,128)(2,1)} %param.31) | copy-start | bytes 1572868
  0.7 33.3 %copy-start.2 = (bf16[128,2048]{1,0:T(8,128)(2,1)S(1)}, bf16[128,2048]{1,0:T(8,128)(2,1)}, u32[]{:S(2)}) copy-start(bf16[128,2048]{1,0:T(8,128)(2,1)} %param.34) | copy-start | bytes 1572868
  30.4 11.7 %copy-start.13 = (s32[16,1]{0,1:T(1,128)S(1)}, s32[16,1]{0,1:T(1,128)}, u32[]{:S(2)}) copy-start(s32[16,1]{0,1:T(1,128)} %param.36) | copy-start | bytes 196
  30.4 12.0 %copy-start.15 = (f32[16,2]{0,1:T(2,128)S(1)}, f32[16,2]{0,1:T(2,128)}, u32[]{:S(2)}) copy-start(f32[16,2]{0,1:T(2,128)} %param.39) | copy-start | bytes 388
  30.4 12.0 %copy-start.17 = (f32[16]{0:T(128)S(1)}, f32[16]{0:T(128)}, u32[]{:S(2)}) copy-start(f32[16]{0:T(128)} %param.38) | copy-start | bytes 196
  30.4 12.1 %copy-start.14 = (s32[16,2]{0,1:T(2,128)S(1)}, s32[16,2]{0,1:T(2,128)}, u32[]{:S(2)}) copy-start(s32[16,2]{0,1:T(2,128)} %param.37) | copy-start | bytes 388
  30.4 20.6 %copy-start.11 = (bf16[16,128]{1,0:T(8,128)(2,1)S(1)}, bf16[16,128]{1,0:T(8,128)(2,1)}, u32[]{:S(2)}) copy-start(bf16[16,128]{1,0:T(8,128)(2,1)} %param.23) | copy-start | bytes 12292
  30.4 32.2 %copy-start.9 = (f32[2048]{0:T(1024)S(1)}, f32[2048]{0:T(1024)}, u32[]{:S(2)}) copy-start(f32[2048]{0:T(1024)} %param.35) | copy-start | bytes 24580
  32.9 29.9 %copy-start.16 = (f32[16]{0:T(128)}, f32[16]{0:T(128)S(1)}, u32[]{:S(2)}) copy-start(f32[16]{0:T(128)S(1)} %fusion.51) | copy-start | bytes 196
  34.0 36.8 %copy-start.10 = (bf16[16,128]{1,0:T(8,128)(2,1)}, bf16[16,128]{1,0:T(8,128)(2,1)S(1)}, u32[]{:S(2)}) copy-start(bf16[16,128]{1,0:T(8,128)(2,1)S(1)} %convolution_convert_fusion.1) | copy-start | bytes 12292
  34.0 36.4 %copy-start.3 = (bf16[128,2048]{1,0:T(8,128)(2,1)S(1)}, bf16[128,2048]{1,0:T(8,128)(2,1)}, u32[]{:S(2)}) copy-start(bf16[128,2048]{1,0:T(8,128)(2,1)} %param.44) | copy-start | bytes 1572868
  34.0 36.4 %copy-start.4 = (bf16[2048,128]{1,0:T(8,128)(2,1)S(1)}, bf16[2048,128]{1,0:T(8,128)(2,1)}, u32[]{:S(2)}) copy-start(bf16[2048,128]{1,0:T(8,128)(2,1)} %param.43) | copy-start | bytes 1572868
  34.3 43.2 %copy-start.5 = (bf16[1,2048,128]{2,1,0:T(8,128)(2,1)S(1)}, bf16[1,2048,128]{2,1,0:T(8,128)(2,1)}, u32[]{:S(2)}) copy-start(bf16[1,2048,128]{2,1,0:T(8,128)(2,1)} %param.40) | copy-start | bytes 1572868
  34.3 43.4 %copy-start.6 = (bf16[1,2048,128]{2,1,0:T(8,128)(2,1)S(1)}, bf16[1,2048,128]{2,1,0:T(8,128)(2,1)}, u32[]{:S(2)}) copy-start(bf16[1,2048,128]{2,1,0:T(8,128)(2,1)} %param.41) | copy-start | bytes 1572868
  37.3 63.6 %copy-start.19 = (f32[128]{0:T(128)S(1)}, f32[128]{0:T(128)}, u32[]{:S(2)}) copy-start(f32[128]{0:T(128)} %param.45) | copy-start | bytes 1540
  38.3 12.7 %all-to-all-start = ((f32[16,16,128]{2,1,0:T(8,128)}), f32[16,16,128]{2,1,0:T(8,128)S(1)}, u32[]{:S(2)}, u32[]{:S(2)}) async-start(f32[16,16,128]{2,1,0:T(8,128)} %convolution_bitcast_fusion), calls=%async_computation | async-start | bytes 262144 | tf_op jit(solution)/shard_map/all_to_all | solution.py:20
  51.6 10.9 %all-to-all-start.1 = ((bf16[16,16,128]{2,1,0:T(8,128)(2,1)}), bf16[16,16,128]{2,1,0:T(8,128)(2,1)S(1)}, u32[]{:S(2)}, u32[]{:S(2)}) async-start(bf16[16,16,128]{2,1,0:T(8,128)(2,1)} %broadcast_in_dim.32), calls=%async_computation.1 | async-start | bytes 131072 | tf_op jit(solution)/shard_map/all_to_all | solution.py:32
  63.6 13.6 %all-to-all-start.2 = ((bf16[16,2,2052]{2,1,0:T(2,128)(2,1)}), bf16[16,2,2052]{2,1,0:T(2,128)(2,1)S(1)}, u32[]{:S(2)}, u32[]{:S(2)}) async-start(bf16[16,2,2052]{2,1,0:T(2,128)(2,1)} %all_to_all.27), calls=%async_computation.2 | async-start | bytes 278528 | tf_op jit(solution)/shard_map/all_to_all | solution.py:42
  97.4 9.9 %all-to-all-start.4 = ((bf16[16,2,128]{2,1,0:T(2,128)(2,1)}), bf16[16,2,128]{2,1,0:T(2,128)(2,1)S(1)}, u32[]{:S(2)}, u32[]{:S(2)}) async-start(bf16[16,2,128]{2,1,0:T(2,128)(2,1)} %bitcast.19), calls=%async_computation.4 | async-start | bytes 16384 | tf_op jit(solution)/shard_map/all_to_all | solution.py:189
where the time goes:
time: 109 us; the launch traced here: 108 us
  blocking collectives  40.5 us (37%)
  waiting for transfers between devices  28.5 us (26%)
  starting transfers between devices  17.4 us (16%)
  matrix products  14.1 us (13%)
  other arithmetic  3.35 us (3%)
  local copies, waits for them, and re-layouts  3.12 us (3%)
    all_gather x1, blocking collectives, body(): gathered = lax.all_gather(tokens, 'tp', axis=1, tiled=True)  21.8 us
    all_to_all x1, blocking collectives, sum_at_owner(): pieces = lax.all_to_all(split_up(array, dim, size), axis, 0, 0, tiled=True)  18.6 us
    all_to_all x1, waiting for transfers between devices, sum_at_owner(): pieces = lax.all_to_all(split_up(array, dim, size), axis, 0, 0, tiled=True)  8.5 us
    all_to_all x1, waiting for transfers between devices, copy_for_each(): return lax.all_to_all(copies, axis, split_axis=0, concat_axis=0, tiled=True)  7.21 us
    all_to_all x1, starting transfers between devices, side_by_side(): lax.all_to_all(both, axis, split_axis=split_dim, concat_axis=concat_dim,...  6.75 us
    all_to_all x1, waiting for transfers between devices, side_by_side(): lax.all_to_all(both, axis, split_axis=split_dim, concat_axis=concat_dim,...  6.44 us
    all_to_all x1, waiting for transfers between devices, body(): lax.all_to_all(expert_sum.astype(jnp.bfloat16), 'ep', split_axis=0, conca...  6.35 us
    all_to_all x1, starting transfers between devices, sum_at_owner(): pieces = lax.all_to_all(split_up(array, dim, size), axis, 0, 0, tiled=True)  3.81 us
  transfers between devices with their start and end apart: 4, of which 4 were waited for; matrix products, arithmetic and copies ran while one was open for 1% of the time, Pallas kernels for 0%

commit v1 on v0

--- a/solution.py
+++ b/solution.py
@@ -118,7 +118,14 @@
     w_dense_out,
     dense_gate,
 ):
-    gathered = lax.all_gather(tokens, "tp", axis=1, tiled=True)
+    size_here = lax.axis_size("tp")
+    gathered = lax.all_to_all(
+        jnp.tile(tokens, tuple((size_here if tick == 1 else 1 for tick in range(tokens.ndim)))),
+        "tp",
+        split_axis=1,
+        concat_axis=1,
+        tiled=True,
+    )
     normed = norm_rows(gathered, attn_gain)
     seq_count = gathered.shape[0]
     heads_dev = key_cache.shape[1]

time: 109 us -> 105 us (0.963)
  blocking collectives: 40.5 us -> 18.6 us
  starting transfers between devices: 17.4 us -> 30.5 us
  other arithmetic: 3.35 us -> 6.91 us
  local copies, waits for them, and re-layouts: 3.12 us -> 6.18 us
  matrix products: 14.1 us -> 12.1 us
    all_gather x1 -> x0, blocking collectives: 21.8 us -> none  [body(): gathered = lax.all_gather(tokens, 'tp', axis=1, tiled=True)]
    all_to_all x0 -> x1, starting transfers between devices: none -> 9.97 us  [body(): lax.all_to_all(jnp.tile(tokens, tuple((size_here if tick == 1 else 1 for...]
    all_to_all x1, starting transfers between devices: 3.81 us -> 6.86 us  [sum_at_owner(): pieces = lax.all_to_all(split_up(array, dim, size), axis, 0, 0, tiled=True)]
    dot_general x1, matrix products: 2.99 us -> 0.72 us  [attend(): jnp.einsum('shl,shld->shd', weights, value_cache, preferred_element_type=...]
    another operation x0 -> x1, local copies, waits for them, and re-layouts: none -> 1.38 us  [body(): jnp.tile(tokens, tuple((size_here if tick == 1 else 1 for tick in range(t...]
  transfers between devices with their start and end apart: 4 -> 5, of which waited for: 4 -> 5; matrix products, arithmetic and copies ran while one was open for 1% -> 8% of each run, Pallas kernels for 0% -> 0%
where the time goes in v1:
time: 105 us
  starting transfers between devices  30.5 us (29%)
  waiting for transfers between devices  29.2 us (28%)
  blocking collectives  18.6 us (18%)
  matrix products  12.1 us (12%)
  other arithmetic  6.91 us (7%)
  local copies, waits for them, and re-layouts  6.18 us (6%)
    all_to_all x1, blocking collectives, sum_at_owner(): pieces = lax.all_to_all(split_up(array, dim, size), axis, 0, 0, tiled=True)  18.6 us
    all_to_all x1, starting transfers between devices, body(): lax.all_to_all(jnp.tile(tokens, tuple((size_here if tick == 1 else 1 for...  9.97 us
    all_to_all x1, waiting for transfers between devices, sum_at_owner(): pieces = lax.all_to_all(split_up(array, dim, size), axis, 0, 0, tiled=True)  8.84 us
    all_to_all x1, waiting for transfers between devices, copy_for_each(): return lax.all_to_all(copies, axis, split_axis=0, concat_axis=0, tiled=True)  7.21 us
    all_to_all x1, starting transfers between devices, sum_at_owner(): pieces = lax.all_to_all(split_up(array, dim, size), axis, 0, 0, tiled=True)  6.86 us
    all_to_all x1, starting transfers between devices, side_by_side(): lax.all_to_all(both, axis, split_axis=split_dim, concat_axis=concat_dim,...  6.75 us
    all_to_all x1, waiting for transfers between devices, side_by_side(): lax.all_to_all(both, axis, split_axis=split_dim, concat_axis=concat_dim,...  6.44 us
    all_to_all x1, waiting for transfers between devices, body(): lax.all_to_all(expert_sum.astype(jnp.bfloat16), 'ep', split_axis=0, conca...  6.35 us
  transfers between devices with their start and end apart: 5, of which 5 were waited for; matrix products, arithmetic and copies ran while one was open for 8% of the time, Pallas kernels for 0%

profile of v1, /device:TPU:1, one launch (start us, length us, event | category | flops | bytes accessed | tf_op | source)
XLA Modules:
  0.0 104.5 jit_solution(7083762711332940347)
XLA Ops:
  0.7 1.4 %tile.2 = bf16[16,16,128]{2,0,1:T(8,128)(2,1)} broadcast(bf16[16,128]{1,0:T(8,128)(2,1)} %param.23), dimensions={0,2} | broadcast | bytes 69632 | tf_op jit(solution)/shard_map/tile | solution.py:123
  2.1 10.0 %all-to-all-start = ((bf16[16,16,128]{2,0,1:T(8,128)(2,1)}), bf16[16,16,128]{2,0,1:T(8,128)(2,1)S(1)}, u32[]{:S(2)}, u32[]{:S(2)}) async-start(bf16[16,16,128]{2,0,1:T(8,128)(2,1)} %tile.2), calls=%async_computation | async-start | bytes 131072 | tf_op jit(solution)/shard_map/all_to_all | solution.py:122
  12.0 0.7 broadcast_add_fusion
  12.7 1.3 %copy.65 = bf16[2048,128]{1,0:T(8,128)(2,1)S(1)} copy(bf16[2048,128]{0,1:T(8,128)(2,1)} %bitcast.127) | data formatting | bytes 1048576 | tf_op jit(solution)/shard_map/dot_general | solution.py:154
  14.0 0.7 fusion.47
  14.8 0.8 select_reduce_fusion.1
  15.6 0.8 broadcast_subtract_fusion
  16.4 1.2 %dynamic_slice.7 = f32[1]{0:T(128)} dynamic-slice(f32[16]{0:T(128)} %param.33, s32[]{:T(128)S(6)} %select_n.34), dynamic_slice_sizes={1} | dynamic-slice | bytes 12 | tf_op jit(solution)/shard_map/dynamic_slice | solution.py:144
  17.6 0.7 maximum_multiply_fusion
  18.3 1.1 %fusion.34 = f32[16]{0:T(128)S(1)} fusion(f32[16,1,1024]{2,1,0:T(1,128)} %param.26, s32[16]{0:T(128)S(1)} %broadcast_add_fusion), kind=kLoop, calls=%fused_computation.53 | loop fusion | flops 49136 | bytes 65664 | tf_op jit(solution)/shard_map/reduce_sum | solution.py:150
  19.9 1.6 %multiply_reduce_fusion.1 = (f32[16]{0:T(128)S(1)}, f32[16,128]{1,0:T(8,128)S(1)}) fusion(bf16[2048,128]{1,0:T(8,128)(2,1)} %param.30, f32[2048]{0:T(1024)} %param.28, f32[16]{0:T(128)S(1)} %add_rsqrt_fusion.3, bf16[16,16,128]{2,0,1:T(8,128)(2,1)S(1)} %all-to-all-done), kind=kOutput, calls=%fused_computation.78 | convolution fusion | flops 8523760 | bytes 606336 | tf_op jit(solution)/shard_map/dot_general | solution.py:135
  21.5 1.4 %multiply_reduce_fusion.2 = (f32[16]{0:T(128)S(1)}, f32[16,128]{1,0:T(8,128)S(1)}) fusion(bf16[2048,128]{1,0:T(8,128)(2,1)} %param.29, f32[2048]{0:T(1024)} %param.28, f32[16]{0:T(128)S(1)} %add_rsqrt_fusion.3, bf16[16,16,128]{2,0,1:T(8,128)(2,1)S(1)} %all-to-all-done), kind=kOutput, calls=%fused_computation.81 | convolution fusion | flops 8523760 | bytes 606336 | tf_op jit(solution)/shard_map/dot_general | solution.py:135
  22.9 0.8 fusion.66
  23.7 3.4 %fusion.2 = f32[16,1,1024]{2,1,0:T(1,128)S(1)} fusion(bf16[16,1,1024,128]{3,2,1,0:T(8,128)(2,1)} %param.24, bf16[16,128,1]{1,0,2:T(8,128)(2,1)S(1)} %get-tuple-element.10), kind=kOutput, calls=%fused_computation.2 | convolution fusion | flops 4194304 | bytes 4263936 | tf_op jit(solution)/shard_map/shd,shld->shl/dot_general | solution.py:73
  27.2 1.7 %fusion.56 = f32[16]{0:T(128)S(1)} fusion(f32[16]{0:T(128)S(1)} %fusion.34, bf16[2048,16]{0,1:T(8,128)(2,1)} %param.32, s32[]{:T(128)S(6)} %select_n.34, f32[]{:T(128)} %bitcast.5, bf16[16,16,128]{2,0,1:T(8,128)(2,1)S(1)} %all-to-all-done, f32[16,128]{1,0:T(8,128)S(1)} %bitcast.128, f32[16]{0:T(128)S(1)} %add_rsqrt_fusion.3), kind=kOutput, calls=%fused_computation.92 | convolution fusion | flops 196768 | bytes 82628 | tf_op jit(solution)/shard_map/dot_general | solution.py:146
  29.7 0.7 fusion
  30.7 0.9 convolution_bitcast_fusion
  31.7 6.9 %all-to-all-start.1 = ((f32[16,16,128]{2,1,0:T(8,128)}), f32[16,16,128]{2,1,0:T(8,128)S(1)}, u32[]{:S(2)}, u32[]{:S(2)}) async-start(f32[16,16,128]{2,1,0:T(8,128)} %convolution_bitcast_fusion), calls=%async_computation.1 | async-start | bytes 262144 | tf_op jit(solution)/shard_map/all_to_all | solution.py:20
  38.6 8.8 %all-to-all-done.1 = f32[16,16,128]{2,1,0:T(8,128)S(1)} async-done(((f32[16,16,128]{2,1,0:T(8,128)}), f32[16,16,128]{2,1,0:T(8,128)S(1)}, u32[]{:S(2)}, u32[]{:S(2)}) %all-to-all-start.1) | async-done | bytes 131104 | tf_op jit(solution)/shard_map/all_to_all | solution.py:20
  47.5 0.6 broadcast_in_dim.32
  48.1 3.4 %all-to-all-start.2 = ((bf16[16,16,128]{2,1,0:T(8,128)(2,1)}), bf16[16,16,128]{2,1,0:T(8,128)(2,1)S(1)}, u32[]{:S(2)}, u32[]{:S(2)}) async-start(bf16[16,16,128]{2,1,0:T(8,128)(2,1)} %broadcast_in_dim.32), calls=%async_computation.2 | async-start | bytes 131072 | tf_op jit(solution)/shard_map/all_to_all | solution.py:32
  51.7 7.2 %all-to-all-done.2 = bf16[16,16,128]{2,1,0:T(8,128)(2,1)S(1)} async-done(((bf16[16,16,128]{2,1,0:T(8,128)(2,1)}), bf16[16,16,128]{2,1,0:T(8,128)(2,1)S(1)}, u32[]{:S(2)}, u32[]{:S(2)}) %all-to-all-start.2) | async-done | bytes 65568 | tf_op jit(solution)/shard_map/all_to_all | solution.py:32
  59.3 0.7 all_to_all.32
  60.0 6.8 %all-to-all-start.3 = ((bf16[16,2,2052]{2,1,0:T(2,128)(2,1)}), bf16[16,2,2052]{2,1,0:T(2,128)(2,1)S(1)}, u32[]{:S(2)}, u32[]{:S(2)}) async-start(bf16[16,2,2052]{2,1,0:T(2,128)(2,1)} %all_to_all.32), calls=%async_computation.3 | async-start | bytes 278528 | tf_op jit(solution)/shard_map/all_to_all | solution.py:42
  66.8 0.4 fusion.49
  67.3 6.4 %all-to-all-done.3 = bf16[16,2,2052]{2,1,0:T(2,128)(2,1)S(1)} async-done(((bf16[16,2,2052]{2,1,0:T(2,128)(2,1)}), bf16[16,2,2052]{2,1,0:T(2,128)(2,1)S(1)}, u32[]{:S(2)}, u32[]{:S(2)}) %all-to-all-start.3) | async-done | bytes 131360 | tf_op jit(solution)/shard_map/all_to_all | solution.py:42
  74.1 0.4 fusion.6
  74.6 18.6 %all_to_all.45 = f32[16,48,128]{2,1,0:T(8,128)S(1)} all-to-all(f32[16,48,128]{2,1,0:T(8,128)S(1)} %bitcast_bitcast_fusion), channel_id=1, replica_groups=mesh['ep'=16,'tp'=16] {'tp'}, dimensions={0} | all-to-all | bytes 786432 | tf_op jit(solution)/shard_map/all_to_all | solution.py:20
  93.2 0.6 split.15
  93.8 3.5 %all-to-all-start.5 = ((bf16[16,2,128]{2,1,0:T(2,128)(2,1)}), bf16[16,2,128]{2,1,0:T(2,128)(2,1)S(1)}, u32[]{:S(2)}, u32[]{:S(2)}) async-start(bf16[16,2,128]{2,1,0:T(2,128)(2,1)} %bitcast.20), calls=%async_computation.5 | async-start | bytes 16384 | tf_op jit(solution)/shard_map/all_to_all | solution.py:196
  97.4 6.3 %all-to-all-done.5 = bf16[16,2,128]{2,1,0:T(2,128)(2,1)S(1)} async-done(((bf16[16,2,128]{2,1,0:T(2,128)(2,1)}), bf16[16,2,128]{2,1,0:T(2,128)(2,1)S(1)}, u32[]{:S(2)}, u32[]{:S(2)}) %all-to-all-start.5) | async-done | bytes 8224 | tf_op jit(solution)/shard_map/all_to_all | solution.py:196
  103.7 0.8 fusion.8
  (62 shorter events, 2.8 us)
Async XLA Ops:
  0.6 73.5 %copy-start = (bf16[1,128,2048]{2,1,0:T(8,128)(2,1)S(1)}, bf16[1,128,2048]{2,1,0:T(8,128)(2,1)}, u32[]{:S(2)}) copy-start(bf16[1,128,2048]{2,1,0:T(8,128)(2,1)} %param.42) | copy-start | bytes 1572868
  0.6 28.4 %copy-start.11 = (s32[16]{0:T(128)S(1)}, s32[16]{0:T(128)}, u32[]{:S(2)}) copy-start(s32[16]{0:T(128)} %param.27) | copy-start | bytes 196
  0.7 28.4 %copy-start.6 = (f32[16,1,1024]{2,1,0:T(1,128)S(1)}, f32[16,1,1024]{2,1,0:T(1,128)}, u32[]{:S(2)}) copy-start(f32[16,1,1024]{2,1,0:T(1,128)} %param.26) | copy-start | bytes 196612
  0.7 26.5 %copy-start.7 = (f32[2048]{0:T(1024)S(1)}, f32[2048]{0:T(1024)}, u32[]{:S(2)}) copy-start(f32[2048]{0:T(1024)} %param.28) | copy-start | bytes 24580
  2.1 17.7 %all-to-all-start = ((bf16[16,16,128]{2,0,1:T(8,128)(2,1)}), bf16[16,16,128]{2,0,1:T(8,128)(2,1)S(1)}, u32[]{:S(2)}, u32[]{:S(2)}) async-start(bf16[16,16,128]{2,0,1:T(8,128)(2,1)} %tile.2), calls=%async_computation | async-start | bytes 131072 | tf_op jit(solution)/shard_map/all_to_all | solution.py:122
  19.8 9.9 %copy-start.15 = (bf16[16,1,1024,128]{3,2,1,0:T(8,128)(2,1)S(1)}, bf16[16,1,1024,128]{3,2,1,0:T(8,128)(2,1)}, u32[]{:S(2)}) copy-start(bf16[16,1,1024,128]{3,2,1,0:T(8,128)(2,1)} %param.25) | copy-start | bytes 12582916
  23.7 6.8 %copy-start.1 = (bf16[2048,128]{1,0:T(8,128)(2,1)S(1)}, bf16[2048,128]{1,0:T(8,128)(2,1)}, u32[]{:S(2)}) copy-start(bf16[2048,128]{1,0:T(8,128)(2,1)} %param.31) | copy-start | bytes 1572868
  27.2 11.4 %copy-start.13 = (s32[16,2]{0,1:T(2,128)S(1)}, s32[16,2]{0,1:T(2,128)}, u32[]{:S(2)}) copy-start(s32[16,2]{0,1:T(2,128)} %param.37) | copy-start | bytes 388
  27.2 11.4 %copy-start.12 = (s32[16,1]{0,1:T(1,128)S(1)}, s32[16,1]{0,1:T(1,128)}, u32[]{:S(2)}) copy-start(s32[16,1]{0,1:T(1,128)} %param.36) | copy-start | bytes 196
  27.2 20.3 %copy-start.10 = (bf16[16,128]{1,0:T(8,128)(2,1)S(1)}, bf16[16,128]{1,0:T(8,128)(2,1)}, u32[]{:S(2)}) copy-start(bf16[16,128]{1,0:T(8,128)(2,1)} %param.23) | copy-start | bytes 12292
  27.2 31.9 %copy-start.8 = (f32[2048]{0:T(1024)S(1)}, f32[2048]{0:T(1024)}, u32[]{:S(2)}) copy-start(f32[2048]{0:T(1024)} %param.35) | copy-start | bytes 24580
  27.2 39.6 %copy-start.2 = (bf16[128,2048]{1,0:T(8,128)(2,1)S(1)}, bf16[128,2048]{1,0:T(8,128)(2,1)}, u32[]{:S(2)}) copy-start(bf16[128,2048]{1,0:T(8,128)(2,1)} %param.44) | copy-start | bytes 1572868
  27.2 39.6 %copy-start.3 = (bf16[2048,128]{1,0:T(8,128)(2,1)S(1)}, bf16[2048,128]{1,0:T(8,128)(2,1)}, u32[]{:S(2)}) copy-start(bf16[2048,128]{1,0:T(8,128)(2,1)} %param.43) | copy-start | bytes 1572868
  28.9 38.3 %copy-start.14 = (f32[16]{0:T(128)}, f32[16]{0:T(128)S(1)}, u32[]{:S(2)}) copy-start(f32[16]{0:T(128)S(1)} %fusion.56) | copy-start | bytes 196
  29.7 44.2 %copy-start.4 = (bf16[1,2048,128]{2,1,0:T(8,128)(2,1)S(1)}, bf16[1,2048,128]{2,1,0:T(8,128)(2,1)}, u32[]{:S(2)}) copy-start(bf16[1,2048,128]{2,1,0:T(8,128)(2,1)} %param.40) | copy-start | bytes 1572868
  29.7 44.4 %copy-start.5 = (bf16[1,2048,128]{2,1,0:T(8,128)(2,1)S(1)}, bf16[1,2048,128]{2,1,0:T(8,128)(2,1)}, u32[]{:S(2)}) copy-start(bf16[1,2048,128]{2,1,0:T(8,128)(2,1)} %param.41) | copy-start | bytes 1572868
  30.7 73.8 %copy-start.9 = (bf16[16,128]{1,0:T(8,128)(2,1)}, bf16[16,128]{1,0:T(8,128)(2,1)S(1)}, u32[]{:S(2)}) copy-start(bf16[16,128]{1,0:T(8,128)(2,1)S(1)} %convolution_convert_fusion.1) | copy-start | bytes 12292
  30.7 66.6 %copy-start.16 = (f32[128]{0:T(128)S(1)}, f32[128]{0:T(128)}, u32[]{:S(2)}) copy-start(f32[128]{0:T(128)} %param.45) | copy-start | bytes 1540
  31.7 15.7 %all-to-all-start.1 = ((f32[16,16,128]{2,1,0:T(8,128)}), f32[16,16,128]{2,1,0:T(8,128)S(1)}, u32[]{:S(2)}, u32[]{:S(2)}) async-start(f32[16,16,128]{2,1,0:T(8,128)} %convolution_bitcast_fusion), calls=%async_computation.1 | async-start | bytes 262144 | tf_op jit(solution)/shard_map/all_to_all | solution.py:20
  48.1 10.9 %all-to-all-start.2 = ((bf16[16,16,128]{2,1,0:T(8,128)(2,1)}), bf16[16,16,128]{2,1,0:T(8,128)(2,1)S(1)}, u32[]{:S(2)}, u32[]{:S(2)}) async-start(bf16[16,16,128]{2,1,0:T(8,128)(2,1)} %broadcast_in_dim.32), calls=%async_computation.2 | async-start | bytes 131072 | tf_op jit(solution)/shard_map/all_to_all | solution.py:32
  60.0 13.6 %all-to-all-start.3 = ((bf16[16,2,2052]{2,1,0:T(2,128)(2,1)}), bf16[16,2,2052]{2,1,0:T(2,128)(2,1)S(1)}, u32[]{:S(2)}, u32[]{:S(2)}) async-start(bf16[16,2,2052]{2,1,0:T(2,128)(2,1)} %all_to_all.32), calls=%async_computation.3 | async-start | bytes 278528 | tf_op jit(solution)/shard_map/all_to_all | solution.py:42
  93.8 9.9 %all-to-all-start.5 = ((bf16[16,2,128]{2,1,0:T(2,128)(2,1)}), bf16[16,2,128]{2,1,0:T(2,128)(2,1)S(1)}, u32[]{:S(2)}, u32[]{:S(2)}) async-start(bf16[16,2,128]{2,1,0:T(2,128)(2,1)} %bitcast.20), calls=%async_computation.5 | async-start | bytes 16384 | tf_op jit(solution)/shard_map/all_to_all | solution.py:196
